TPU v7x, 32 devices: a whole 2x2x4 slice. The times are simulated.
32 devices in a mesh: kv: 8 (over z, x), tp: 4 (over y, core).
Axes of the slice: x: 2, y: 2, z: 4, core: 2. Of those that a mesh axis runs over, the one named last changes fastest.
Arguments:
- tokens: bfloat16 [1024, 2048], P('kv'), may hold values from -64 to 64
- query_weight: bfloat16 [2048, 1024], P(None, 'tp'), may hold values from -0.125 to 0.125
- key_weight: bfloat16 [2048, 256], P(None, 'tp'), may hold values from -0.125 to 0.125
- value_weight: bfloat16 [2048, 256], P(None, 'tp'), may hold values from -0.125 to 0.125
- out_weight: bfloat16 [1024, 2048], P(None, 'tp'), may hold values from -0.1875 to 0.1875
- alibi_slope: float32 [16], P('tp'), may hold values from 0.00024414062 to 0.03
- block_choice: int32 [32, 8], P('kv'), may hold values from -1 to 31, as said below
Outputs:
- mixed: bfloat16 [1024, 2048], P('kv', 'tp')
Inputs may be any that keep to these rules, and one draw needn't show every extreme that they name: `block_choice`: row g begins with g; its other entries are distinct blocks below g, or -1 where nothing is chosen. The rows of one index of kv (aligned runs of 4 rows) together name at most one block of any other index of kv, and some rows of each index name a block of the index before it and of the index half the axis before it where those exist.
All inputs are finite; a program needn't handle non-finite values.
Results may differ from a plain program's by a relative error of at most 0.012.
Values may be sent and summed in bfloat16 or wider, within the bound.
A program may use at most 64 MiB of HBM per device.

v0:
```python
import jax
import jax.numpy as jnp
from jax import lax
from jax.sharding import PartitionSpec as P

HEAD = 64
BLOCK = 32


def shards(tokens, query_weight, key_weight, value_weight, out_weight, alibi_slope, block_choice):
    rows = tokens.shape[0]
    blocks_here = rows // BLOCK
    n_kv = lax.axis_size("kv")
    device = lax.axis_index("kv")
    queries = jnp.dot(tokens, query_weight, preferred_element_type=jnp.float32).astype(jnp.bfloat16)
    keys = jnp.dot(tokens, key_weight, preferred_element_type=jnp.float32).astype(jnp.bfloat16)
    values = jnp.dot(tokens, value_weight, preferred_element_type=jnp.float32).astype(jnp.bfloat16)
    packed = jnp.concatenate([keys, values], axis=1)
    safe_ids = jnp.maximum(block_choice, 0)
    owners = safe_ids // blocks_here
    local_index = safe_ids % blocks_here
    remote = (block_choice >= 0) & (owners != device)
    match = remote[..., None] & (owners[..., None] == jnp.arange(n_kv, dtype=jnp.int32))
    wanted = jnp.max(jnp.where(match, local_index[..., None], -1), axis=(0, 1))
    own_blocks = packed.reshape(blocks_here, BLOCK, 2 * HEAD)
    asked = lax.all_to_all(wanted.reshape(n_kv, 1), "kv", split_axis=0, concat_axis=0, tiled=True)
    outgoing = own_blocks[jnp.clip(asked[:, 0], 0, blocks_here - 1)]
    incoming = lax.all_to_all(outgoing, "kv", split_axis=0, concat_axis=0, tiled=True)
    table = jnp.concatenate([own_blocks, incoming], axis=0)
    slot_ids = jnp.where(owners == device, local_index, blocks_here + owners)
    selected = table[slot_ids]
    heads_here = queries.shape[1] // HEAD
    query_blocks = queries.reshape(blocks_here, BLOCK, heads_here, HEAD)
    block_ids = device * blocks_here + jnp.arange(blocks_here, dtype=jnp.int32)
    scale = HEAD ** (-0.5)

    def attend(args):
        query_blk, picked, chosen, block_id, safe_row = args
        scores = (
            jnp.einsum(
                "qhd,nkd->hqnk", query_blk, picked[..., :HEAD], preferred_element_type=jnp.float32
            )
            * scale
        )
        query_pos = block_id * BLOCK + jnp.arange(BLOCK, dtype=jnp.int32)
        key_pos = safe_row[:, None] * BLOCK + jnp.arange(BLOCK, dtype=jnp.int32)[None, :]
        distance = query_pos[:, None, None] - key_pos[None, :, :]
        scores = scores - alibi_slope[:, None, None, None] * distance.astype(jnp.float32)[None]
        keep = (chosen >= 0)[None, :, None] & (distance >= 0)
        scores = jnp.where(keep[None], scores, -jnp.inf)
        weights = jax.nn.softmax(scores, axis=(2, 3)).astype(jnp.bfloat16)
        attended = jnp.einsum(
            "hqnk,nkd->qhd", weights, picked[..., HEAD:], preferred_element_type=jnp.float32
        )
        return attended.astype(jnp.bfloat16).reshape(BLOCK, heads_here * HEAD)

    attended = lax.map(attend, (query_blocks, selected, block_choice, block_ids, safe_ids))
    attended = attended.reshape(rows, heads_here * HEAD)
    result = jnp.dot(
        lax.all_gather(attended, "tp", axis=1, tiled=True),
        out_weight,
        preferred_element_type=jnp.float32,
    )
    return result.astype(jnp.bfloat16)


def solution(mesh):
    in_specs = (
        P("kv", None),
        P(None, "tp"),
        P(None, "tp"),
        P(None, "tp"),
        P(None, "tp"),
        P("tp"),
        P("kv", None),
    )
    out_specs = P("kv", "tp")
    return jax.shard_map(shards, mesh=mesh, in_specs=in_specs, out_specs=out_specs, check_vma=False)
```

profile of v0, /device:TPU:0, one launch (start us, length us, event | category | flops | bytes accessed | tf_op | source)
XLA Modules:
  0.0 48.2 jit_solution(8471632134200029447)
XLA Ops:
  0.0 0.8 %broadcast_maximum_fusion = (s32[4,8]{1,0:T(4,128)S(1)}, s32[4,8]{1,0:T(4,128)S(1)}, s32[4,8]{1,0:T(4,128)S(1)}, s32[4,8]{1,0:T(4,128)S(1)}) fusion(s32[4,8]{1,0:T(4,128)} %param.15, s32[]{:T(128)S(6)} %axis_index.15), kind=kLoop, calls=%fused_computation.48 | loop fusion | flops 608 | bytes 644 | tf_op jit(solution)/shard_map/max | solution.py:19
  0.9 0.7 %compare_and_fusion = pred[4,8]{1,0:T(4,128)(4,1)S(1)} fusion(s32[4,8]{1,0:T(4,128)} %param.15, s32[]{:T(128)S(6)} %axis_index.15), kind=kLoop, calls=%fused_computation.46 | loop fusion | flops 384 | bytes 164 | tf_op jit(solution)/shard_map/and | solution.py:22
  1.6 0.7 %copy.28 = s32[8,1,1]{2,1,0:T(1,128)} copy(s32[8,1,1]{0,2,1:T(1,128)S(1)} %bitcast.80) | data formatting | bytes 64 | tf_op jit(solution)/shard_map/all_to_all | solution.py:26
  2.3 7.3 %all-to-all-start = ((s32[8,1,1]{2,1,0:T(1,128)}), s32[8,1,1]{2,1,0:T(1,128)S(1)}, u32[]{:S(2)}, u32[]{:S(2)}) async-start(s32[8,1,1]{2,1,0:T(1,128)} %copy.28), calls=%async_computation | async-start | bytes 8192 | tf_op jit(solution)/shard_map/all_to_all | solution.py:26
  9.6 1.4 %convolution_convert_fusion.2 = bf16[128,64]{0,1:T(8,128)(2,1)S(1)} fusion(bf16[128,2048]{1,0:T(8,128)(2,1)} %param.9, bf16[2048,64]{0,1:T(8,128)(2,1)} %param.12), kind=kOutput, calls=%fused_computation.30 | convolution fusion | flops 33562624 | bytes 802816 | tf_op jit(solution)/shard_map/dot_general | solution.py:17
  11.0 1.2 %convolution_convert_fusion.3 = bf16[128,64]{0,1:T(8,128)(2,1)S(1)} fusion(bf16[128,2048]{1,0:T(8,128)(2,1)S(1)} %copy-done.1, bf16[2048,64]{0,1:T(8,128)(2,1)} %param.11), kind=kOutput, calls=%fused_computation.31 | convolution fusion | flops 33562624 | bytes 802816 | tf_op jit(solution)/shard_map/dot_general | solution.py:16
  12.4 0.3 convolution_convert_fusion.1
  12.7 3.3 %all-to-all-done = s32[8,1,1]{2,1,0:T(1,128)S(1)} async-done(((s32[8,1,1]{2,1,0:T(1,128)}), s32[8,1,1]{2,1,0:T(1,128)S(1)}, u32[]{:S(2)}, u32[]{:S(2)}) %all-to-all-start) | async-done | bytes 64 | tf_op jit(solution)/shard_map/all_to_all | solution.py:26
  16.3 1.2 %gather_fusion = bf16[8,32,128]{2,1,0:T(8,128)(2,1)} fusion(bf16[4,32,128]{2,1,0:T(8,128)(2,1)S(1)} %bitcast.77, s32[1024]{0:T(1024)S(1)} %pad_clamp_fusion.1), kind=kCustom, calls=%fused_computation | custom fusion | bytes 131104 | tf_op jit(solution)/shard_map/gather | solution.py:27
  17.5 3.4 %all-to-all-start.1 = ((bf16[8,32,128]{2,1,0:T(8,128)(2,1)}), bf16[8,32,128]{2,1,0:T(8,128)(2,1)S(1)}, u32[]{:S(2)}, u32[]{:S(2)}) async-start(bf16[8,32,128]{2,1,0:T(8,128)(2,1)} %gather_fusion), calls=%async_computation.1 | async-start | bytes 131072 | tf_op jit(solution)/shard_map/all_to_all | solution.py:28
  21.1 6.6 %all-to-all-done.1 = bf16[8,32,128]{2,1,0:T(8,128)(2,1)S(1)} async-done(((bf16[8,32,128]{2,1,0:T(8,128)(2,1)}), bf16[8,32,128]{2,1,0:T(8,128)(2,1)S(1)}, u32[]{:S(2)}, u32[]{:S(2)}) %all-to-all-start.1) | async-done | bytes 65568 | tf_op jit(solution)/shard_map/all_to_all | solution.py:28
  27.7 0.6 %gather_fusion.1 = bf16[32,32,128]{2,1,0:T(8,128)(2,1)S(1)} fusion(bf16[12,32,128]{2,1,0:T(8,128)(2,1)S(1)} %pad_maximum_fusion, s32[1024]{0:T(1024)S(1)} %pad_clamp_fusion), kind=kCustom, calls=%fused_computation.1 | custom fusion | bytes 524416 | tf_op jit(solution)/shard_map/gather | solution.py:31
  28.3 0.6 %copy-done.3 = f32[4]{0:T(128)S(1)} copy-done((f32[4]{0:T(128)S(1)}, f32[4]{0:T(128)}, u32[]{:S(2)}) %copy-start.3) | copy-done | bytes 40
  29.0 12.5 %while.10 = (s32[]{:T(128)}, bf16[4,32,256]{2,1,0:T(8,128)(2,1)S(1)}, bf16[4,8,32,128]{3,2,1,0:T(8,128)(2,1)S(1)}, s32[4,8]{1,0:T(4,128)}, s32[4]{0:T(128)S(1)},...) while((s32[]{:T(128)}, ...), condition=%wide.region_4.5_spmd, body=%wide.region_1.4_spmd.sunk | while | flops 8765491 | bytes 907445 | solution.py:57
  29.0 0.6 %dynamic_slice.38 = s32[1]{0:T(128)} dynamic-slice(s32[4]{0:T(128)S(1)} %get-tuple-element.187, s32[]{:T(128)} %get-tuple-element.173), dynamic_slice_sizes={1} | dynamic-slice | bytes 12 | tf_op jit(solution)/shard_map/while/body/jit(dynamic_index_in_dim)/dynamic_slice | solution.py:57
  30.3 0.7 %compare_bitcast_fusion.2 = pred[8]{0:T(512)(128)(4,1)S(1)} fusion(s32[4,8]{1,0:T(4,128)} %get-tuple-element.186, s32[]{:T(128)} %get-tuple-element.173), kind=kLoop, calls=%fused_computation.20.clone.1 | loop fusion | flops 8 | bytes 44 | tf_op jit(solution)/shard_map/while/body/eval_jaxpr/ge | solution.py:49
  31.3 0.3 fusion.28
  31.7 0.3 fusion.30
  32.1 0.6 %dynamic_slice.38 = s32[1]{0:T(128)} dynamic-slice(s32[4]{0:T(128)S(1)} %get-tuple-element.187, s32[]{:T(128)} %get-tuple-element.173), dynamic_slice_sizes={1} | dynamic-slice | bytes 12 | tf_op jit(solution)/shard_map/while/body/jit(dynamic_index_in_dim)/dynamic_slice | solution.py:57
  33.4 0.7 %compare_bitcast_fusion.2 = pred[8]{0:T(512)(128)(4,1)S(1)} fusion(s32[4,8]{1,0:T(4,128)} %get-tuple-element.186, s32[]{:T(128)} %get-tuple-element.173), kind=kLoop, calls=%fused_computation.20.clone.1 | loop fusion | flops 8 | bytes 44 | tf_op jit(solution)/shard_map/while/body/eval_jaxpr/ge | solution.py:49
  34.4 0.3 fusion.28
  34.8 0.3 fusion.30
  35.2 0.6 %dynamic_slice.38 = s32[1]{0:T(128)} dynamic-slice(s32[4]{0:T(128)S(1)} %get-tuple-element.187, s32[]{:T(128)} %get-tuple-element.173), dynamic_slice_sizes={1} | dynamic-slice | bytes 12 | tf_op jit(solution)/shard_map/while/body/jit(dynamic_index_in_dim)/dynamic_slice | solution.py:57
  36.6 0.7 %compare_bitcast_fusion.2 = pred[8]{0:T(512)(128)(4,1)S(1)} fusion(s32[4,8]{1,0:T(4,128)} %get-tuple-element.186, s32[]{:T(128)} %get-tuple-element.173), kind=kLoop, calls=%fused_computation.20.clone.1 | loop fusion | flops 8 | bytes 44 | tf_op jit(solution)/shard_map/while/body/eval_jaxpr/ge | solution.py:49
  37.5 0.3 fusion.28
  37.9 0.3 fusion.30
  38.3 0.6 %dynamic_slice.38 = s32[1]{0:T(128)} dynamic-slice(s32[4]{0:T(128)S(1)} %get-tuple-element.187, s32[]{:T(128)} %get-tuple-element.173), dynamic_slice_sizes={1} | dynamic-slice | bytes 12 | tf_op jit(solution)/shard_map/while/body/jit(dynamic_index_in_dim)/dynamic_slice | solution.py:57
  39.7 0.7 %compare_bitcast_fusion.2 = pred[8]{0:T(512)(128)(4,1)S(1)} fusion(s32[4,8]{1,0:T(4,128)} %get-tuple-element.186, s32[]{:T(128)} %get-tuple-element.173), kind=kLoop, calls=%fused_computation.20.clone.1 | loop fusion | flops 8 | bytes 44 | tf_op jit(solution)/shard_map/while/body/eval_jaxpr/ge | solution.py:49
  40.7 0.3 fusion.28
  41.1 0.3 fusion.30
  41.5 5.8 %all_gather.3 = bf16[128,1024]{1,0:T(8,128)(2,1)S(1)} all-gather(bf16[128,256]{1,0:T(8,128)(2,1)S(1)} %bitcast.79), channel_id=1, replica_groups=mesh['kv'=8,'tp'=4] {'tp'}, dimensions={1}, use_global_device_ids=true | all-gather | bytes 327680 | tf_op jit(solution)/shard_map/all_gather | solution.py:60
  47.3 1.0 %convolution_convert_fusion = bf16[128,512]{1,0:T(8,128)(2,1)} fusion(bf16[128,1024]{1,0:T(8,128)(2,1)S(1)} %all_gather.3, bf16[1024,512]{1,0:T(8,128)(2,1)S(1)} %copy-done), kind=kOutput, calls=%fused_computation.28 | convolution fusion | flops 134283264 | bytes 1441792 | tf_op jit(solution)/shard_map/dot_general | solution.py:59
  (63 shorter events, 3.0 us)
Async XLA Ops:
  0.0 47.3 %copy-start = (bf16[1024,512]{1,0:T(8,128)(2,1)S(1)}, bf16[1024,512]{1,0:T(8,128)(2,1)}, u32[]{:S(2)}) copy-start(bf16[1024,512]{1,0:T(8,128)(2,1)} %param.13) | copy-start | bytes 3145732
  0.0 11.0 %copy-start.1 = (bf16[128,2048]{1,0:T(8,128)(2,1)S(1)}, bf16[128,2048]{1,0:T(8,128)(2,1)}, u32[]{:S(2)}) copy-start(bf16[128,2048]{1,0:T(8,128)(2,1)} %param.9) | copy-start | bytes 1572868
  0.0 12.4 %copy-start.2 = (bf16[2048,256]{1,0:T(8,128)(2,1)S(1)}, bf16[2048,256]{1,0:T(8,128)(2,1)}, u32[]{:S(2)}) copy-start(bf16[2048,256]{1,0:T(8,128)(2,1)} %param.10) | copy-start | bytes 3145732
  2.3 13.7 %all-to-all-start = ((s32[8,1,1]{2,1,0:T(1,128)}), s32[8,1,1]{2,1,0:T(1,128)S(1)}, u32[]{:S(2)}, u32[]{:S(2)}) async-start(s32[8,1,1]{2,1,0:T(1,128)} %copy.28), calls=%async_computation | async-start | bytes 8192 | tf_op jit(solution)/shard_map/all_to_all | solution.py:26
  17.5 10.2 %all-to-all-start.1 = ((bf16[8,32,128]{2,1,0:T(8,128)(2,1)}), bf16[8,32,128]{2,1,0:T(8,128)(2,1)S(1)}, u32[]{:S(2)}, u32[]{:S(2)}) async-start(bf16[8,32,128]{2,1,0:T(8,128)(2,1)} %gather_fusion), calls=%async_computation.1 | async-start | bytes 131072 | tf_op jit(solution)/shard_map/all_to_all | solution.py:28
  28.3 0.7 %copy-start.3 = (f32[4]{0:T(128)S(1)}, f32[4]{0:T(128)}, u32[]{:S(2)}) copy-start(f32[4]{0:T(128)} %param.14) | copy-start | bytes 52
where the time goes:
time: 48.7 us; the launch traced here: 48.2 us
  starting transfers between devices  10.6 us (22%)
  waiting for transfers between devices  9.88 us (20%)
  local copies, waits for them, and re-layouts  6.44 us (13%)
  other arithmetic  6.3 us (13%)
  matrix products  6.16 us (13%)
  blocking collectives  5.78 us (12%)
  loops' own time  2.89 us (6%)
    all_to_all x1, starting transfers between devices, shards(): lax.all_to_all(wanted.reshape(n_kv, 1), 'kv', split_axis=0, concat_axis=0...  7.29 us
    all_to_all x1, waiting for transfers between devices, shards(): lax.all_to_all(outgoing, 'kv', split_axis=0, concat_axis=0, tiled=True)  6.6 us
    all_gather x1, blocking collectives, shards(): lax.all_gather(attended, 'tp', axis=1, tiled=True)  5.78 us
    all_to_all x1, starting transfers between devices, shards(): lax.all_to_all(outgoing, 'kv', split_axis=0, concat_axis=0, tiled=True)  3.35 us
    all_to_all x1, waiting for transfers between devices, shards(): lax.all_to_all(wanted.reshape(n_kv, 1), 'kv', split_axis=0, concat_axis=0...  3.28 us
    another operation x1, loops' own time, shards(): lax.map(attend, (query_blocks, selected, block_choice, block_ids, safe_ids))  2.89 us
    ge x4, other arithmetic, attend(): keep = (chosen >= 0)[None, :, None] & (distance >= 0)  2.76 us
    dynamic_slice x8, local copies, waits for them, and re-layouts, shards(): lax.map(attend, (query_blocks, selected, block_choice, block_ids, safe_ids))  2.43 us
  transfers between devices with their start and end apart: 2, of which 2 were waited for; matrix products, arithmetic and copies ran while one was open for 7% of the time, Pallas kernels for 0%

commit v1 on v0

v1 whole, which is shorter than its diff:
```python
import functools

import jax
import jax.numpy as jnp
from jax import lax
from jax.experimental import pallas as pl
from jax.experimental.pallas import tpu as pltpu
from jax.sharding import PartitionSpec as P

HEAD = 64
BLOCK = 32
LANES = 2 * HEAD
FULL_FROM = 64
NEVER = 1 << 28


def each(low, high, body):
    if high - low <= 16:
        for i in range(low, high):
            body(i)
    else:
        pl.loop(low, high)(body)


def kernel(n_kv, n_tp, tok_hbm, wq_hbm, wk_hbm, wv_hbm, wo_hbm, slope, choice, choice_vec,
           out, tok, wq, wkv, wo, table, want_out, want_in, send_buf, q_pad, bias, att,
           load_sem, want_send, want_recv, kv_send, kv_recv, att_send, att_recv):
    me = lax.axis_index("kv")
    mt = lax.axis_index("tp")
    rows = tok.shape[0]
    nb = rows // BLOCK
    heads = wq.shape[1] // HEAD
    topk = choice.shape[1]
    picked = topk * BLOCK
    stacked = heads * BLOCK

    loads = [
        pltpu.make_async_copy(tok_hbm, tok, load_sem.at[0]),
        pltpu.make_async_copy(wk_hbm, wkv.at[pl.ds(0, HEAD)], load_sem.at[1]),
        pltpu.make_async_copy(wv_hbm, wkv.at[pl.ds(HEAD, HEAD)], load_sem.at[2]),
        pltpu.make_async_copy(wq_hbm, wq, load_sem.at[3]),
        pltpu.make_async_copy(wo_hbm, wo, load_sem.at[4]),
    ]
    barrier = pltpu.get_barrier_semaphore()
    each(1, n_kv, lambda k: pl.semaphore_signal(
        barrier, inc=1, device_id={"kv": lax.rem(me + k, n_kv)}))
    for d in range(1, n_tp):
        pl.semaphore_signal(barrier, inc=1, device_id={"tp": lax.rem(mt + d, n_tp)})
    for load in loads:
        load.start()

    ids = choice_vec[...]
    owner = ids // nb
    local = ids - owner * nb

    def note_want(k):
        hit = (ids >= 0) & (owner == me - k)
        found = jnp.max(jnp.where(hit, local, -1).astype(jnp.float32), keepdims=True)
        want_out[k] = jnp.broadcast_to(found, (8, LANES))

    each(1, min(n_kv, FULL_FROM) if n_kv <= 16 else n_kv, note_want)

    for load in loads[:3]:
        load.wait()
    kv = lax.dot_general(tok[...], wkv[...], (((1,), (1,)), ((), ())),
                         preferred_element_type=jnp.float32).astype(jnp.bfloat16)
    table[pl.ds(0, nb)] = kv.reshape(nb, BLOCK, LANES)

    pl.semaphore_wait(barrier, n_kv - 1 + n_tp - 1)

    def wanted_only(k):
        return n_kv > 16 or k < FULL_FROM

    def want_copy(k):
        return pltpu.make_async_remote_copy(
            src_ref=want_out.at[k], dst_ref=want_in.at[k],
            send_sem=want_send.at[k], recv_sem=want_recv.at[k],
            device_id={"kv": lax.rem(me - k + n_kv, n_kv)})

    def kv_copy(k):
        whole = not wanted_only(k)
        return pltpu.make_async_remote_copy(
            src_ref=table.at[pl.ds(0, nb)] if whole else send_buf.at[k],
            dst_ref=table.at[pl.ds(k * nb, nb)] if whole else table.at[k * nb],
            send_sem=kv_send.at[k], recv_sem=kv_recv.at[k],
            device_id={"kv": lax.rem(me + k, n_kv)})

    def first_sends(k):
        if wanted_only(k):
            @pl.when(me - k >= 0)
            def _():
                want_copy(k).start()
        else:
            @pl.when(me + k < n_kv)
            def _():
                kv_copy(k).start()

    if n_kv <= 16:
        for k in reversed(range(1, n_kv)):
            first_sends(k)
    else:
        each(1, n_kv, first_sends)

    lane = lax.broadcasted_iota(jnp.int32, (1, LANES), 1)
    low = lane < HEAD
    loads[3].wait()
    queries = jnp.dot(tok[...], wq[...], preferred_element_type=jnp.float32)
    queries = queries * (HEAD ** -0.5)
    for pair in range(heads // 2):
        two = queries[:, pair * LANES:(pair + 1) * LANES]
        swapped = pltpu.roll(two, HEAD, 1)
        for half, part in enumerate((two, swapped)):
            part = jnp.where(low, part, 0.0).astype(jnp.bfloat16)
            head = 2 * pair + half
            for g in range(nb):
                q_pad[g, head * BLOCK:(head + 1) * BLOCK, :] = part[g * BLOCK:(g + 1) * BLOCK]

    def answer(k):
        if wanted_only(k):
            @pl.when(me + k < n_kv)
            def _():
                want_copy(k).wait_recv()
                want = want_in[k]
                chosen = jnp.zeros((BLOCK // 8, 8, LANES), jnp.float32)
                for b in range(nb):
                    blk = table[b].astype(jnp.float32).reshape(BLOCK // 8, 8, LANES)
                    chosen = jnp.where((want == float(b))[None], blk, chosen)
                send_buf[k] = chosen.reshape(BLOCK, LANES).astype(jnp.bfloat16)
                kv_copy(k).start()

    each(1, n_kv, answer)

    row = lax.broadcasted_iota(jnp.int32, (stacked, 1), 0)
    slope_col = jnp.zeros((stacked, 1), jnp.float32)
    for h in range(heads):
        slope_col = jnp.where(row // BLOCK == h, slope[h], slope_col)
    q_in = lax.rem(row, BLOCK)
    col = lax.broadcasted_iota(jnp.int32, (1, picked), 1)
    rows_of = []
    for g in range(nb):
        base = jnp.zeros((1, picked), jnp.int32)
        here = []
        for j in range(topk):
            c = choice[g, j]
            base = jnp.where(col // BLOCK == j, jnp.where(c < 0, NEVER, c * BLOCK), base)
            safe = jnp.where(c < 0, me * nb, c)
            own = safe // nb
            k = me - own
            loc = safe - own * nb
            exact = k == 0
            if n_kv <= 16:
                exact = exact | (k >= FULL_FROM)
            here.append(k * nb + jnp.where(exact, loc, 0))
        rows_of.append(here)
        key_pos = base + lax.rem(col, BLOCK)
        dist = ((me * nb + g) * BLOCK + q_in) - key_pos
        bias[g] = jnp.where(dist >= 0, -slope_col * dist.astype(jnp.float32), -jnp.inf)

    def kv_arrived(k):
        @pl.when(me - k >= 0)
        def _():
            kv_copy(k).wait_recv()

    each(1, n_kv, kv_arrived)

    keep_hi = jnp.where(low, 0.0, 1.0).astype(jnp.bfloat16)
    ones_lo = jnp.where(low, 1.0, 0.0).astype(jnp.bfloat16)

    partner = mt + 1 - 2 * lax.rem(mt, 2)
    peers = [partner]
    for i in range(2, n_tp, 2):
        peers += [lax.rem(mt + i, n_tp), lax.rem(partner + i, n_tp)]

    def att_copy(p, g, source):
        piece = att.at[source, pl.ds(g * BLOCK, BLOCK)]
        return pltpu.make_async_remote_copy(
            src_ref=piece, dst_ref=piece,
            send_sem=att_send.at[p, g], recv_sem=att_recv.at[source, g],
            device_id={"tp": peers[p]})

    for g in range(nb):
        chosen = jnp.concatenate([table[r] for r in rows_of[g]], axis=0)
        scores = lax.dot_general(q_pad[g], chosen, (((1,), (1,)), ((), ())),
                                 preferred_element_type=jnp.float32) + bias[g]
        top = jnp.max(scores, axis=1, keepdims=True)
        weights = jnp.exp(scores - top).astype(jnp.bfloat16)
        got = jnp.dot(weights, chosen * keep_hi + ones_lo, preferred_element_type=jnp.float32)
        turned = pltpu.roll(got, HEAD, 1)
        for pair in range(heads // 2):
            even = slice(2 * pair * BLOCK, (2 * pair + 1) * BLOCK)
            odd = slice((2 * pair + 1) * BLOCK, (2 * pair + 2) * BLOCK)
            num = jnp.where(low, turned[even], got[odd])
            den = jnp.where(low, got[even], turned[odd])
            att[mt, pl.ds(g * BLOCK, BLOCK), pl.ds(pair * LANES, LANES)] = (num / den).astype(jnp.bfloat16)
        for p in reversed(range(n_tp - 1)):
            att_copy(p, g, mt).start()

    width = heads * HEAD

    def term(source):
        return jnp.dot(att[source], wo[pl.ds(source * width, width)],
                       preferred_element_type=jnp.float32)

    loads[4].wait()
    total = term(mt)
    for p in range(n_tp - 1):
        for g in range(nb):
            att_copy(p, g, peers[p]).wait_recv()
        total += term(peers[p])
    out[...] = total.astype(out.dtype)

    def finish(k):
        if wanted_only(k):
            @pl.when(me - k >= 0)
            def _():
                want_copy(k).wait_send()

        @pl.when(me + k < n_kv)
        def _():
            kv_copy(k).wait_send()

    each(1, n_kv, finish)
    for p in range(n_tp - 1):
        for g in range(nb):
            att_copy(p, g, mt).wait_send()


def shards(n_kv, n_tp, tokens, query_weight, key_weight, value_weight, out_weight, alibi_slope, block_choice):
    rows, depth = tokens.shape
    nb = rows // BLOCK
    width = query_weight.shape[1]
    heads = width // HEAD
    topk = block_choice.shape[1]
    hbm = pl.BlockSpec(memory_space=pltpu.HBM)
    smem = pl.BlockSpec(memory_space=pltpu.SMEM)
    vmem = pl.BlockSpec(memory_space=pltpu.VMEM)
    bf16 = jnp.bfloat16
    dma = pltpu.SemaphoreType.DMA
    return pl.pallas_call(
        functools.partial(kernel, n_kv, n_tp),
        out_shape=jax.ShapeDtypeStruct((rows, out_weight.shape[1]), bf16),
        in_specs=[hbm] * 5 + [smem, smem, vmem],
        out_specs=vmem,
        scratch_shapes=[
            pltpu.VMEM((rows, depth), bf16),
            pltpu.VMEM((depth, width), bf16),
            pltpu.VMEM((LANES, depth), bf16),
            pltpu.VMEM(out_weight.shape, bf16),
            pltpu.VMEM((n_kv * nb, BLOCK, LANES), bf16),
            pltpu.VMEM((n_kv, 8, LANES), jnp.float32),
            pltpu.VMEM((n_kv, 8, LANES), jnp.float32),
            pltpu.VMEM((n_kv, BLOCK, LANES), bf16),
            pltpu.VMEM((nb, heads * BLOCK, LANES), bf16),
            pltpu.VMEM((nb, heads * BLOCK, topk * BLOCK), jnp.float32),
            pltpu.VMEM((n_tp, rows, width), bf16),
            dma((5,)),
            dma((n_kv,)),
            dma((n_kv,)),
            dma((n_kv,)),
            dma((n_kv,)),
            dma((n_tp - 1, nb)),
            dma((n_tp, nb)),
        ],
        compiler_params=pltpu.CompilerParams(collective_id=0, has_side_effects=True),
    )(tokens, query_weight, key_weight.T, value_weight.T, out_weight, alibi_slope, block_choice, block_choice)


def solution(mesh):
    in_specs = (
        P("kv", None),
        P(None, "tp"),
        P(None, "tp"),
        P(None, "tp"),
        P(None, "tp"),
        P("tp"),
        P("kv", None),
    )
    body = functools.partial(shards, mesh.shape["kv"], mesh.shape["tp"])
    return jax.shard_map(body, mesh=mesh, in_specs=in_specs, out_specs=P("kv", "tp"), check_vma=False)
```

time: 48.7 us -> 19.2 us (0.39)
  the two profiles are of different devices: /device:TPU:0 before, /device:TPU:24 now
where the time goes in v1:
time: 19.2 us; the launch traced here: 19 us
  Pallas kernels  17.4 us (91%)
  local copies, waits for them, and re-layouts  1.57 us (8%)
    pallas_call x1, Pallas kernels, shards(): pl.pallas_call(functools.partial(kernel, n_kv, n_tp), out_shape=jax.Shape...  17.4 us
    unnamed x1, local copies, waits for them, and re-layouts  1.57 us

profile of v1, /device:TPU:24, one launch (start us, length us, event | category | flops | bytes accessed | tf_op | source)
XLA Modules:
  0.0 19.0 jit_solution(4912724048021354046)
XLA Ops:
  0.0 17.4 %shard_map.73 = bf16[128,512]{1,0:T(8,128)(2,1)} custom-call(bf16[128,2048]{1,0:T(8,128)(2,1)} %tok_hbm.1, bf16[2048,256]{1,0:T(8,128)(2,1)} %wq_hbm.1, bf16[64,2048]{1,0:T(8,128)(2,1)} %bitcast.2, bf16[64,2048]{1,0:T(8,128)(2,1)} %bitcast.3, bf16[1024,512]{1,0:T(8,128)(2,1)} %wo_hbm.1, f32[4]{0:T(128)} %slope.1, s32[4,8]{1,0:T(4,128)} %choice_vec.1, ...), custom_call_target="tpu_custom_call" | custom-call | tf_op jit(solution)/shard_map/pallas_call | solution.py:239
  17.4 1.6 %copy.9 = bf16[128,512]{1,0:T(8,128)(2,1)} copy(bf16[128,512]{1,0:T(8,128)(2,1)} %shard_map.73) | data formatting | bytes 262144

commit v2 on v1

--- a/solution.py
+++ b/solution.py
@@ -12,6 +12,7 @@
 LANES = 2 * HEAD
 FULL_FROM = 64
 NEVER = 1 << 28
+GROUP = 2
 
 
 def each(low, high, body):
@@ -22,8 +23,8 @@
         pl.loop(low, high)(body)
 
 
-def kernel(n_kv, n_tp, tok_hbm, wq_hbm, wk_hbm, wv_hbm, wo_hbm, slope, choice, choice_vec,
-           out, tok, wq, wkv, wo, table, want_out, want_in, send_buf, q_pad, bias, att,
+def kernel(n_kv, n_tp, tok_hbm, wq_hbm, wk_hbm, wv_hbm, wo_hbm, slope_hbm, choice_hbm,
+           out, slope, choice, choice_vec, tok, wq, wkv, wo, table, want_out, want_in, send_buf, q_pad, bias, att,
            load_sem, want_send, want_recv, kv_send, kv_recv, att_send, att_recv):
     me = lax.axis_index("kv")
     mt = lax.axis_index("tp")
@@ -41,14 +42,20 @@
         pltpu.make_async_copy(wq_hbm, wq, load_sem.at[3]),
         pltpu.make_async_copy(wo_hbm, wo, load_sem.at[4]),
     ]
+    small = [
+        pltpu.make_async_copy(choice_hbm, choice_vec, load_sem.at[5]),
+        pltpu.make_async_copy(choice_hbm, choice, load_sem.at[6]),
+        pltpu.make_async_copy(slope_hbm, slope, load_sem.at[7]),
+    ]
     barrier = pltpu.get_barrier_semaphore()
     each(1, n_kv, lambda k: pl.semaphore_signal(
         barrier, inc=1, device_id={"kv": lax.rem(me + k, n_kv)}))
     for d in range(1, n_tp):
         pl.semaphore_signal(barrier, inc=1, device_id={"tp": lax.rem(mt + d, n_tp)})
-    for load in loads:
+    for load in small + loads:
         load.start()
 
+    small[0].wait()
     ids = choice_vec[...]
     owner = ids // nb
     local = ids - owner * nb
@@ -59,14 +66,6 @@
         want_out[k] = jnp.broadcast_to(found, (8, LANES))
 
     each(1, min(n_kv, FULL_FROM) if n_kv <= 16 else n_kv, note_want)
-
-    for load in loads[:3]:
-        load.wait()
-    kv = lax.dot_general(tok[...], wkv[...], (((1,), (1,)), ((), ())),
-                         preferred_element_type=jnp.float32).astype(jnp.bfloat16)
-    table[pl.ds(0, nb)] = kv.reshape(nb, BLOCK, LANES)
-
-    pl.semaphore_wait(barrier, n_kv - 1 + n_tp - 1)
 
     def wanted_only(k):
         return n_kv > 16 or k < FULL_FROM
@@ -85,21 +84,24 @@
             send_sem=kv_send.at[k], recv_sem=kv_recv.at[k],
             device_id={"kv": lax.rem(me + k, n_kv)})
 
-    def first_sends(k):
+    def ask(k):
         if wanted_only(k):
             @pl.when(me - k >= 0)
             def _():
                 want_copy(k).start()
-        else:
-            @pl.when(me + k < n_kv)
-            def _():
-                kv_copy(k).start()
-
-    if n_kv <= 16:
-        for k in reversed(range(1, n_kv)):
-            first_sends(k)
-    else:
-        each(1, n_kv, first_sends)
+
+    def meet():
+        pl.semaphore_wait(barrier, n_kv - 1 + n_tp - 1)
+        each(1, n_kv, ask)
+
+    early = me * 2 >= n_kv
+    pl.when(early)(meet)
+
+    for load in loads[:3]:
+        load.wait()
+    kv = lax.dot_general(tok[...], wkv[...], (((1,), (1,)), ((), ())),
+                         preferred_element_type=jnp.float32).astype(jnp.bfloat16)
+    table[pl.ds(0, nb)] = kv.reshape(nb, BLOCK, LANES)
 
     lane = lax.broadcasted_iota(jnp.int32, (1, LANES), 1)
     low = lane < HEAD
@@ -128,8 +130,19 @@
                 send_buf[k] = chosen.reshape(BLOCK, LANES).astype(jnp.bfloat16)
                 kv_copy(k).start()
 
+    pl.when(jnp.logical_not(early))(meet)
+
+    def send_all(k):
+        if not wanted_only(k):
+            @pl.when(me + k < n_kv)
+            def _():
+                kv_copy(k).start()
+
+    each(1, n_kv, send_all)
     each(1, n_kv, answer)
 
+    small[1].wait()
+    small[2].wait()
     row = lax.broadcasted_iota(jnp.int32, (stacked, 1), 0)
     slope_col = jnp.zeros((stacked, 1), jnp.float32)
     for h in range(heads):
@@ -178,7 +191,7 @@
             send_sem=att_send.at[p, g], recv_sem=att_recv.at[source, g],
             device_id={"tp": peers[p]})
 
-    for g in range(nb):
+    def attend(g):
         chosen = jnp.concatenate([table[r] for r in rows_of[g]], axis=0)
         scores = lax.dot_general(q_pad[g], chosen, (((1,), (1,)), ((), ())),
                                  preferred_element_type=jnp.float32) + bias[g]
@@ -186,14 +199,23 @@
         weights = jnp.exp(scores - top).astype(jnp.bfloat16)
         got = jnp.dot(weights, chosen * keep_hi + ones_lo, preferred_element_type=jnp.float32)
         turned = pltpu.roll(got, HEAD, 1)
+        parts = []
         for pair in range(heads // 2):
             even = slice(2 * pair * BLOCK, (2 * pair + 1) * BLOCK)
             odd = slice((2 * pair + 1) * BLOCK, (2 * pair + 2) * BLOCK)
             num = jnp.where(low, turned[even], got[odd])
             den = jnp.where(low, got[even], turned[odd])
-            att[mt, pl.ds(g * BLOCK, BLOCK), pl.ds(pair * LANES, LANES)] = (num / den).astype(jnp.bfloat16)
-        for p in reversed(range(n_tp - 1)):
-            att_copy(p, g, mt).start()
+            parts.append((num / den).astype(jnp.bfloat16))
+        return jnp.concatenate(parts, axis=1)
+
+    for first in range(0, nb, GROUP):
+        group = range(first, min(first + GROUP, nb))
+        done = [attend(g) for g in group]
+        for g, value in zip(group, done):
+            att[mt, pl.ds(g * BLOCK, BLOCK), :] = value
+        for g in group:
+            for p in reversed(range(n_tp - 1)):
+                att_copy(p, g, mt).start()
 
     width = heads * HEAD
 
@@ -232,16 +254,18 @@
     heads = width // HEAD
     topk = block_choice.shape[1]
     hbm = pl.BlockSpec(memory_space=pltpu.HBM)
-    smem = pl.BlockSpec(memory_space=pltpu.SMEM)
     vmem = pl.BlockSpec(memory_space=pltpu.VMEM)
     bf16 = jnp.bfloat16
     dma = pltpu.SemaphoreType.DMA
     return pl.pallas_call(
         functools.partial(kernel, n_kv, n_tp),
-        out_shape=jax.ShapeDtypeStruct((rows, out_weight.shape[1]), bf16),
-        in_specs=[hbm] * 5 + [smem, smem, vmem],
+        out_shape=pltpu.VMEM((rows, out_weight.shape[1]), bf16),
+        in_specs=[hbm] * 7,
         out_specs=vmem,
         scratch_shapes=[
+            pltpu.SMEM(alibi_slope.shape, jnp.float32),
+            pltpu.SMEM(block_choice.shape, jnp.int32),
+            pltpu.VMEM(block_choice.shape, jnp.int32),
             pltpu.VMEM((rows, depth), bf16),
             pltpu.VMEM((depth, width), bf16),
             pltpu.VMEM((LANES, depth), bf16),
@@ -253,7 +277,7 @@
             pltpu.VMEM((nb, heads * BLOCK, LANES), bf16),
             pltpu.VMEM((nb, heads * BLOCK, topk * BLOCK), jnp.float32),
             pltpu.VMEM((n_tp, rows, width), bf16),
-            dma((5,)),
+            dma((8,)),
             dma((n_kv,)),
             dma((n_kv,)),
             dma((n_kv,)),
@@ -262,7 +286,7 @@
             dma((n_tp, nb)),
         ],
         compiler_params=pltpu.CompilerParams(collective_id=0, has_side_effects=True),
-    )(tokens, query_weight, key_weight.T, value_weight.T, out_weight, alibi_slope, block_choice, block_choice)
+    )(tokens, query_weight, key_weight.T, value_weight.T, out_weight, alibi_slope, block_choice)
 
 
 def solution(mesh):

time: 19.2 us -> 16.5 us (0.86)
  Pallas kernels: 17.4 us -> 15.7 us
  local copies, waits for them, and re-layouts: 1.57 us -> 0.66 us
    pallas_call x1, Pallas kernels: 17.4 us -> 15.7 us  [shards(): pl.pallas_call(functools.partial(kernel, n_kv, n_tp), out_shape=pltpu.VME...]
    unnamed x1, local copies, waits for them, and re-layouts: 1.57 us -> 0.66 us
where the time goes in v2:
time: 16.5 us; the launch traced here: 16.3 us
  Pallas kernels  15.7 us (95%)
  local copies, waits for them, and re-layouts  0.66 us (4%)
    pallas_call x1, Pallas kernels, shards(): pl.pallas_call(functools.partial(kernel, n_kv, n_tp), out_shape=pltpu.VME...  15.7 us
    unnamed x1, local copies, waits for them, and re-layouts  0.66 us

profile of v2, /device:TPU:24, one launch (start us, length us, event | category | flops | bytes accessed | tf_op | source)
XLA Modules:
  0.0 16.3 jit_solution(6214449875079980082)
XLA Ops:
  0.0 15.7 %shard_map.73 = bf16[128,512]{1,0:T(8,128)(2,1)S(1)} custom-call(bf16[128,2048]{1,0:T(8,128)(2,1)} %tok_hbm.1, bf16[2048,256]{1,0:T(8,128)(2,1)} %wq_hbm.1, bf16[64,2048]{1,0:T(8,128)(2,1)} %bitcast.2, bf16[64,2048]{1,0:T(8,128)(2,1)} %bitcast.3, bf16[1024,512]{1,0:T(8,128)(2,1)} %wo_hbm.1, f32[4]{0:T(128)} %slope_hbm.1, s32[4,8]{1,0:T(4,128)} %choice_hbm.1), custom_call_target="tpu_custom_call" | custom-call | tf_op jit(solution)/shard_map/pallas_call | solution.py:260
  15.7 0.7 %copy.9 = bf16[128,512]{1,0:T(8,128)(2,1)} copy(bf16[128,512]{1,0:T(8,128)(2,1)S(1)} %shard_map.73) | data formatting | bytes 262144

commit v3 on v2

--- a/solution.py
+++ b/solution.py
@@ -10,8 +10,10 @@
 HEAD = 64
 BLOCK = 32
 LANES = 2 * HEAD
-FULL_FROM = 64
 NEVER = 1 << 28
+RELAY = 0
+FAR = 3
+SMALL = 16
 GROUP = 2
 
 
@@ -23,9 +25,19 @@
         pl.loop(low, high)(body)
 
 
+def when(*conditions):
+    if any(c is False for c in conditions):
+        return lambda body: None
+    return pl.when(functools.reduce(jnp.logical_and, [c for c in conditions if c is not True]))
+
+
+def negate(condition):
+    return not condition if isinstance(condition, bool) else jnp.logical_not(condition)
+
+
 def kernel(n_kv, n_tp, tok_hbm, wq_hbm, wk_hbm, wv_hbm, wo_hbm, slope_hbm, choice_hbm,
            out, slope, choice, choice_vec, tok, wq, wkv, wo, table, want_out, want_in, send_buf, q_pad, bias, att,
-           load_sem, want_send, want_recv, kv_send, kv_recv, att_send, att_recv):
+           load_sem, want_send, want_recv, kv_send, kv_recv, att_send, att_recv, fwd_send):
     me = lax.axis_index("kv")
     mt = lax.axis_index("tp")
     rows = tok.shape[0]
@@ -48,8 +60,22 @@
         pltpu.make_async_copy(slope_hbm, slope, load_sem.at[7]),
     ]
     barrier = pltpu.get_barrier_semaphore()
-    each(1, n_kv, lambda k: pl.semaphore_signal(
-        barrier, inc=1, device_id={"kv": lax.rem(me + k, n_kv)}))
+
+    def far(k, owner):
+        if n_kv > SMALL or (k + 1) // 2 < FAR:
+            return False
+        return True if k // 2 >= FAR else lax.rem(owner, 2) == 1
+
+    def greet(k):
+        @pl.when(me + k < n_kv)
+        def _():
+            pl.semaphore_signal(barrier, inc=1, device_id={"kv": lax.rem(me + k, n_kv)})
+
+        @when(far(k, me + k), me - k >= 0)
+        def _():
+            pl.semaphore_signal(barrier, inc=1, device_id={"kv": lax.rem(me - k + n_kv, n_kv)})
+
+    each(1, n_kv, greet)
     for d in range(1, n_tp):
         pl.semaphore_signal(barrier, inc=1, device_id={"tp": lax.rem(mt + d, n_tp)})
     for load in small + loads:
@@ -65,10 +91,7 @@
         found = jnp.max(jnp.where(hit, local, -1).astype(jnp.float32), keepdims=True)
         want_out[k] = jnp.broadcast_to(found, (8, LANES))
 
-    each(1, min(n_kv, FULL_FROM) if n_kv <= 16 else n_kv, note_want)
-
-    def wanted_only(k):
-        return n_kv > 16 or k < FULL_FROM
+    each(1, n_kv, note_want)
 
     def want_copy(k):
         return pltpu.make_async_remote_copy(
@@ -76,26 +99,35 @@
             send_sem=want_send.at[k], recv_sem=want_recv.at[k],
             device_id={"kv": lax.rem(me - k + n_kv, n_kv)})
 
-    def kv_copy(k):
-        whole = not wanted_only(k)
+    def kv_copy(k, unasked=False):
         return pltpu.make_async_remote_copy(
-            src_ref=table.at[pl.ds(0, nb)] if whole else send_buf.at[k],
-            dst_ref=table.at[pl.ds(k * nb, nb)] if whole else table.at[k * nb],
+            src_ref=table.at[pl.ds(0, nb)] if unasked else send_buf.at[k],
+            dst_ref=table.at[pl.ds(k * nb, nb)] if unasked else table.at[k * nb],
             send_sem=kv_send.at[k], recv_sem=kv_recv.at[k],
             device_id={"kv": lax.rem(me + k, n_kv)})
 
     def ask(k):
-        if wanted_only(k):
-            @pl.when(me - k >= 0)
-            def _():
-                want_copy(k).start()
+        @when(negate(far(k, me + k)), me - k >= 0)
+        def _():
+            want_copy(k).start()
+
+    far_peers = 0
+    if n_kv <= SMALL:
+        for k in range(1, n_kv):
+            mine = far(k, me)
+            if mine is not False:
+                mine = (me + k < n_kv) if mine is True else mine & (me + k < n_kv)
+                far_peers += jnp.where(mine, 1, 0)
 
     def meet():
-        pl.semaphore_wait(barrier, n_kv - 1 + n_tp - 1)
+        pl.semaphore_wait(barrier, me + far_peers + n_tp - 1)
         each(1, n_kv, ask)
 
-    early = me * 2 >= n_kv
-    pl.when(early)(meet)
+    early = far_peers == 0
+    if n_kv <= SMALL:
+        pl.when(early)(meet)
+    else:
+        meet()
 
     for load in loads[:3]:
         load.wait()
@@ -117,28 +149,28 @@
             for g in range(nb):
                 q_pad[g, head * BLOCK:(head + 1) * BLOCK, :] = part[g * BLOCK:(g + 1) * BLOCK]
 
+    if n_kv <= SMALL:
+        pl.when(jnp.logical_not(early))(meet)
+
+    def send_all(k):
+        @when(far(k, me), me + k < n_kv)
+        def _():
+            kv_copy(k, True).start()
+
+    each(1, n_kv, send_all)
+
     def answer(k):
-        if wanted_only(k):
-            @pl.when(me + k < n_kv)
-            def _():
-                want_copy(k).wait_recv()
-                want = want_in[k]
-                chosen = jnp.zeros((BLOCK // 8, 8, LANES), jnp.float32)
-                for b in range(nb):
-                    blk = table[b].astype(jnp.float32).reshape(BLOCK // 8, 8, LANES)
-                    chosen = jnp.where((want == float(b))[None], blk, chosen)
-                send_buf[k] = chosen.reshape(BLOCK, LANES).astype(jnp.bfloat16)
-                kv_copy(k).start()
-
-    pl.when(jnp.logical_not(early))(meet)
-
-    def send_all(k):
-        if not wanted_only(k):
-            @pl.when(me + k < n_kv)
-            def _():
-                kv_copy(k).start()
-
-    each(1, n_kv, send_all)
+        @when(negate(far(k, me)), me + k < n_kv)
+        def _():
+            want_copy(k).wait_recv()
+            want = want_in[k]
+            chosen = jnp.zeros((BLOCK // 8, 8, LANES), jnp.float32)
+            for b in range(nb):
+                blk = table[b].astype(jnp.float32).reshape(BLOCK // 8, 8, LANES)
+                chosen = jnp.where((want == float(b))[None], blk, chosen)
+            send_buf[k] = chosen.reshape(BLOCK, LANES).astype(jnp.bfloat16)
+            kv_copy(k).start()
+
     each(1, n_kv, answer)
 
     small[1].wait()
@@ -161,8 +193,8 @@
             k = me - own
             loc = safe - own * nb
             exact = k == 0
-            if n_kv <= 16:
-                exact = exact | (k >= FULL_FROM)
+            if n_kv <= SMALL:
+                exact = exact | (me // 2 - own // 2 >= FAR)
             here.append(k * nb + jnp.where(exact, loc, 0))
         rows_of.append(here)
         key_pos = base + lax.rem(col, BLOCK)
@@ -170,9 +202,12 @@
         bias[g] = jnp.where(dist >= 0, -slope_col * dist.astype(jnp.float32), -jnp.inf)
 
     def kv_arrived(k):
-        @pl.when(me - k >= 0)
-        def _():
-            kv_copy(k).wait_recv()
+        for unasked in (False, True):
+            kind = far(k, me + k)
+
+            @when(kind if unasked else negate(kind), me - k >= 0)
+            def _():
+                kv_copy(k, unasked).wait_recv()
 
     each(1, n_kv, kv_arrived)
 
@@ -190,6 +225,16 @@
             src_ref=piece, dst_ref=piece,
             send_sem=att_send.at[p, g], recv_sem=att_recv.at[source, g],
             device_id={"tp": peers[p]})
+
+    def relayed(p, g):
+        return p >= 2 and p % 2 == 0 and g < RELAY
+
+    def forward(p, g):
+        piece = att.at[peers[p], pl.ds(g * BLOCK, BLOCK)]
+        return pltpu.make_async_remote_copy(
+            src_ref=piece, dst_ref=piece,
+            send_sem=fwd_send.at[p, g], recv_sem=att_recv.at[peers[p], g],
+            device_id={"tp": partner})
 
     def attend(g):
         chosen = jnp.concatenate([table[r] for r in rows_of[g]], axis=0)
@@ -215,7 +260,8 @@
             att[mt, pl.ds(g * BLOCK, BLOCK), :] = value
         for g in group:
             for p in reversed(range(n_tp - 1)):
-                att_copy(p, g, mt).start()
+                if not relayed(p, g):
+                    att_copy(p, g, mt).start()
 
     width = heads * HEAD
 
@@ -225,26 +271,36 @@
 
     loads[4].wait()
     total = term(mt)
+    for g in range(min(RELAY, nb)):
+        for p in range(1, n_tp - 1, 2):
+            att_copy(p, g, peers[p]).wait_recv()
+            forward(p, g).start()
     for p in range(n_tp - 1):
         for g in range(nb):
-            att_copy(p, g, peers[p]).wait_recv()
+            if not (p % 2 == 1 and g < RELAY):
+                att_copy(p, g, peers[p]).wait_recv()
         total += term(peers[p])
     out[...] = total.astype(out.dtype)
 
     def finish(k):
-        if wanted_only(k):
-            @pl.when(me - k >= 0)
+        @when(negate(far(k, me + k)), me - k >= 0)
+        def _():
+            want_copy(k).wait_send()
+
+        for unasked in (False, True):
+            kind = far(k, me)
+
+            @when(kind if unasked else negate(kind), me + k < n_kv)
             def _():
-                want_copy(k).wait_send()
-
-        @pl.when(me + k < n_kv)
-        def _():
-            kv_copy(k).wait_send()
+                kv_copy(k, unasked).wait_send()
 
     each(1, n_kv, finish)
     for p in range(n_tp - 1):
         for g in range(nb):
-            att_copy(p, g, mt).wait_send()
+            if not relayed(p, g):
+                att_copy(p, g, mt).wait_send()
+            if p % 2 == 1 and g < RELAY:
+                forward(p, g).wait_send()
 
 
 def shards(n_kv, n_tp, tokens, query_weight, key_weight, value_weight, out_weight, alibi_slope, block_choice):
@@ -284,6 +340,7 @@
             dma((n_kv,)),
             dma((n_tp - 1, nb)),
             dma((n_tp, nb)),
+            dma((n_tp - 1, nb)),
         ],
         compiler_params=pltpu.CompilerParams(collective_id=0, has_side_effects=True),
     )(tokens, query_weight, key_weight.T, value_weight.T, out_weight, alibi_slope, block_choice)

time: 16.5 us -> 15.7 us (0.952)
  the two profiles are of different devices: /device:TPU:24 before, /device:TPU:18 now
where the time goes in v3:
time: 15.7 us; the launch traced here: 15.6 us
  Pallas kernels  14.9 us (95%)
  local copies, waits for them, and re-layouts  0.66 us (4%)
    pallas_call x1, Pallas kernels, shards(): pl.pallas_call(functools.partial(kernel, n_kv, n_tp), out_shape=pltpu.VME...  14.9 us
    unnamed x1, local copies, waits for them, and re-layouts  0.66 us

profile of v3, /device:TPU:18, one launch (start us, length us, event | category | flops | bytes accessed | tf_op | source)
XLA Modules:
  0.0 15.6 jit_solution(6424760744839574540)
XLA Ops:
  0.0 14.9 %shard_map.73 = bf16[128,512]{1,0:T(8,128)(2,1)S(1)} custom-call(bf16[128,2048]{1,0:T(8,128)(2,1)} %tok_hbm.1, bf16[2048,256]{1,0:T(8,128)(2,1)} %wq_hbm.1, bf16[64,2048]{1,0:T(8,128)(2,1)} %bitcast.2, bf16[64,2048]{1,0:T(8,128)(2,1)} %bitcast.3, bf16[1024,512]{1,0:T(8,128)(2,1)} %wo_hbm.1, f32[4]{0:T(128)} %slope_hbm.1, s32[4,8]{1,0:T(4,128)} %choice_hbm.1), custom_call_target="tpu_custom_call" | custom-call | tf_op jit(solution)/shard_map/pallas_call | solution.py:316
  14.9 0.7 %copy.9 = bf16[128,512]{1,0:T(8,128)(2,1)} copy(bf16[128,512]{1,0:T(8,128)(2,1)S(1)} %shard_map.73) | data formatting | bytes 262144

commit v4 on v3

--- a/solution.py
+++ b/solution.py
@@ -44,6 +44,8 @@
     nb = rows // BLOCK
     heads = wq.shape[1] // HEAD
     topk = choice.shape[1]
+    step = GROUP if nb % GROUP == 0 else 1
+    pieces = nb // step
     picked = topk * BLOCK
     stacked = heads * BLOCK
 
@@ -220,7 +222,7 @@
         peers += [lax.rem(mt + i, n_tp), lax.rem(partner + i, n_tp)]
 
     def att_copy(p, g, source):
-        piece = att.at[source, pl.ds(g * BLOCK, BLOCK)]
+        piece = att.at[source, pl.ds(g * step * BLOCK, step * BLOCK)]
         return pltpu.make_async_remote_copy(
             src_ref=piece, dst_ref=piece,
             send_sem=att_send.at[p, g], recv_sem=att_recv.at[source, g],
@@ -230,7 +232,7 @@
         return p >= 2 and p % 2 == 0 and g < RELAY
 
     def forward(p, g):
-        piece = att.at[peers[p], pl.ds(g * BLOCK, BLOCK)]
+        piece = att.at[peers[p], pl.ds(g * step * BLOCK, step * BLOCK)]
         return pltpu.make_async_remote_copy(
             src_ref=piece, dst_ref=piece,
             send_sem=fwd_send.at[p, g], recv_sem=att_recv.at[peers[p], g],
@@ -253,15 +255,14 @@
             parts.append((num / den).astype(jnp.bfloat16))
         return jnp.concatenate(parts, axis=1)
 
-    for first in range(0, nb, GROUP):
-        group = range(first, min(first + GROUP, nb))
+    for first in range(0, nb, step):
+        group = range(first, first + step)
         done = [attend(g) for g in group]
         for g, value in zip(group, done):
             att[mt, pl.ds(g * BLOCK, BLOCK), :] = value
-        for g in group:
-            for p in reversed(range(n_tp - 1)):
-                if not relayed(p, g):
-                    att_copy(p, g, mt).start()
+        for p in reversed(range(n_tp - 1)):
+            if not relayed(p, first // step):
+                att_copy(p, first // step, mt).start()
 
     width = heads * HEAD
 
@@ -271,16 +272,20 @@
 
     loads[4].wait()
     total = term(mt)
-    for g in range(min(RELAY, nb)):
+    for g in range(min(RELAY, pieces)):
         for p in range(1, n_tp - 1, 2):
             att_copy(p, g, peers[p]).wait_recv()
             forward(p, g).start()
-    for p in range(n_tp - 1):
-        for g in range(nb):
+    span = step * BLOCK
+    for g in range(pieces):
+        here = slice(g * span, (g + 1) * span)
+        part = total[here]
+        for p in range(n_tp - 1):
             if not (p % 2 == 1 and g < RELAY):
                 att_copy(p, g, peers[p]).wait_recv()
-        total += term(peers[p])
-    out[...] = total.astype(out.dtype)
+            part += jnp.dot(att[peers[p], here, :], wo[pl.ds(peers[p] * width, width)],
+                            preferred_element_type=jnp.float32)
+        out[here, :] = part.astype(out.dtype)
 
     def finish(k):
         @when(negate(far(k, me + k)), me - k >= 0)
@@ -296,7 +301,7 @@
 
     each(1, n_kv, finish)
     for p in range(n_tp - 1):
-        for g in range(nb):
+        for g in range(pieces):
             if not relayed(p, g):
                 att_copy(p, g, mt).wait_send()
             if p % 2 == 1 and g < RELAY:

time: 15.7 us -> 15.6 us (level)
  no operation moved by 1% of the time
where the time goes in v4:
time: 15.6 us; the launch traced here: 15.5 us
  Pallas kernels  14.8 us (95%)
  local copies, waits for them, and re-layouts  0.66 us (4%)
    pallas_call x1, Pallas kernels, shards(): pl.pallas_call(functools.partial(kernel, n_kv, n_tp), out_shape=pltpu.VME...  14.8 us
    unnamed x1, local copies, waits for them, and re-layouts  0.66 us

profile of v4, /device:TPU:18, one launch (start us, length us, event | category | flops | bytes accessed | tf_op | source)
XLA Modules:
  0.0 15.5 jit_solution(3061333853704197548)
XLA Ops:
  0.0 14.8 %shard_map.73 = bf16[128,512]{1,0:T(8,128)(2,1)S(1)} custom-call(bf16[128,2048]{1,0:T(8,128)(2,1)} %tok_hbm.1, bf16[2048,256]{1,0:T(8,128)(2,1)} %wq_hbm.1, bf16[64,2048]{1,0:T(8,128)(2,1)} %bitcast.2, bf16[64,2048]{1,0:T(8,128)(2,1)} %bitcast.3, bf16[1024,512]{1,0:T(8,128)(2,1)} %wo_hbm.1, f32[4]{0:T(128)} %slope_hbm.1, s32[4,8]{1,0:T(4,128)} %choice_hbm.1), custom_call_target="tpu_custom_call" | custom-call | tf_op jit(solution)/shard_map/pallas_call | solution.py:321
  14.8 0.7 %copy.9 = bf16[128,512]{1,0:T(8,128)(2,1)} copy(bf16[128,512]{1,0:T(8,128)(2,1)S(1)} %shard_map.73) | data formatting | bytes 262144
